TPU v7x, 32 devices: a whole 2x2x4 slice. The times are simulated.
32 devices in a mesh: ep: 32 (over z, y, x, core).
Axes of the slice: x: 2, y: 2, z: 4, core: 2. Of those that a mesh axis runs over, the one named last changes fastest.
Arguments:
- tokens: bfloat16 [8192, 2048], P('ep'), may hold values from -6 to 6
- norm_gain: float32 [2048], replicated, may hold values from 0.1 to 1.9
- expert_ids: int32 [8192, 2], P('ep'), may hold values from 0 to 31, as said below
- gates: float32 [8192, 2], P('ep'), may hold values from 0.1 to 1
- w_gate: bfloat16 [32, 2048, 1024], P('ep'), may hold values from -0.125 to 0.125
- w_up: bfloat16 [32, 2048, 1024], P('ep'), may hold values from -0.125 to 0.125
- w_down: bfloat16 [32, 1024, 2048], P('ep'), may hold values from -0.1875 to 0.1875
Outputs:
- combined: bfloat16 [8192, 2048], P('ep')
Inputs may be any that keep to these rules, and one draw needn't show every extreme that they name: `expert_ids`: each row names two different experts of one group, a group being 4 consecutive expert numbers. Among the rows of one device no expert is named more than 32 times, and some expert is named exactly 32 times; some expert is named exactly 32 times by the rows of every device.
All inputs are finite; a program needn't handle non-finite values.
Results may differ from a plain program's by a relative error of at most 0.0085.
Values may be sent and summed in bfloat16 or wider, within the bound.
A program may use at most 128 MiB of HBM per device.

v0:
```python
import functools

import jax
import jax.numpy as jnp
from jax import lax
from jax.experimental import pallas as pl
from jax.experimental.pallas import tpu as pltpu
from jax.sharding import PartitionSpec as P

EPS = 1e-06
MEMBERS = 4
FFN_LAG = 1
MIX_LAG = 2
LANES = 128
MESH = pl.DeviceIdType.MESH
F32 = jnp.float32
BF16 = jnp.bfloat16


def xor(a, b, count):
    total, bit = 0, 1
    while bit < count:
        total = total + ((a // bit + b // bit) % 2) * bit
        bit *= 2
    return total


def steps_in_order(groups):
    upper = list(range(groups // 2, groups))
    lower = list(range(1, groups // 2))
    middle = []
    while upper or lower:
        middle += lower[:1] + upper[:2]
        lower, upper = lower[1:], upper[2:]
    return [0, *middle]


def sends_in_order(groups):
    return steps_in_order(groups)[1:]


def entry(table, t):
    return sum(jnp.where(t == k, value, 0) for k, value in enumerate(table))


def merge_rows(block):
    parts, rows, width = block.shape
    if rows % 16 == 0:
        return block.reshape(parts * rows, width)
    return block.astype(F32).reshape(parts * rows, width).astype(BF16)


def split_rows(block, parts):
    rows, width = block.shape
    return block.reshape(parts, rows // parts, width).astype(BF16)


def chunks(width, size):
    size = min(width, size)
    return [slice(start, start + size) for start in range(0, width, size)]


def dot(a, b):
    return jnp.dot(a, b, preferred_element_type=F32)


def kernel(
    groups, cap,
    ids_ref, gates_ref, tokens_ref, gain_ref, wg_hbm, wu_hbm, wd_hbm, out_ref,
    wg, wu, wd, normed, pack, pack_meta, blk, meta, sel, rows, hidden, outs, obuf, comb, back,
    w_sem, s1_send, s1_recv, m_send, m_recv, s2_send, s2_recv, r2_send, r2_recv, r1_send, r1_recv,
):
    tok, width = tokens_ref.shape
    ff = wg.shape[1]
    slots = 2 * cap
    experts = groups * MEMBERS
    me = lax.axis_index("ep")
    group, member = me // MEMBERS, me % MEMBERS

    loads = [
        pltpu.make_async_copy(src.at[0], dst, w_sem.at[k])
        for k, (src, dst) in enumerate(((wg_hbm, wg), (wu_hbm, wu), (wd_hbm, wd)))
    ]
    for load in loads:
        load.start()

    def far(i):
        return xor(group, i, groups) * MEMBERS + member

    def near(k):
        return group * MEMBERS + xor(member, k, MEMBERS)

    barrier = pltpu.get_barrier_semaphore()
    for k in range(1, MEMBERS):
        pl.semaphore_signal(barrier, inc=1, device_id=(near(k),), device_id_type=MESH)

    @pl.loop(1, groups)
    def _(i):
        pl.semaphore_signal(barrier, inc=1, device_id=(far(i),), device_id_type=MESH)

    for r in range(0, tok, 64):
        part = pl.ds(r, min(64, tok))
        floats = tokens_ref[part, :].astype(F32)
        inverse = lax.rsqrt(jnp.mean(floats * floats, axis=-1, keepdims=True) + EPS)
        normed[part, :] = (floats * inverse * gain_ref[...]).astype(BF16)

    ids = ids_ref[...]
    first, second = ids[0:1, :], ids[1:2, :]
    before = (
        lax.broadcasted_iota(jnp.int32, (tok, tok), 0) < lax.broadcasted_iota(jnp.int32, (tok, tok), 1)
    ).astype(F32).astype(BF16)
    expert_iota = lax.broadcasted_iota(jnp.int32, (experts, tok), 0)
    is_first = (expert_iota == first).astype(F32)
    is_second = (expert_iota == second).astype(F32)
    earlier = dot((is_first + is_second).astype(BF16), before)
    place_first = jnp.sum(earlier * is_first, axis=0, keepdims=True) + 1.0
    place_second = jnp.sum(earlier * is_second, axis=0, keepdims=True) + 1.0
    token_group = first // MEMBERS
    group_rows = max(groups, 8)
    is_group = (lax.broadcasted_iota(jnp.int32, (group_rows, tok), 0) == token_group).astype(F32)
    slot = jnp.sum(dot(is_group.astype(BF16), before) * is_group, axis=0, keepdims=True).astype(jnp.int32)
    step_of = xor(token_group, jnp.full_like(token_group, group), groups)
    key = step_of * slots + slot

    local_first, local_second = first % MEMBERS, second % MEMBERS
    gates = gates_ref[...]
    gate_high = gates.astype(BF16).astype(F32)
    gate_low = (gates - gate_high).astype(BF16).astype(F32)

    def member_rows(of_first, of_second):
        m = lax.broadcasted_iota(jnp.int32, (8, tok), 0)
        return jnp.where(m == local_first, of_first, 0.0) + jnp.where(m == local_second, of_second, 0.0)

    facts = jnp.concatenate(
        [
            member_rows(place_first, place_second),
            member_rows(gate_high[0:1, :], gate_high[1:2, :]),
            member_rows(gate_low[0:1, :], gate_low[1:2, :]),
            jnp.zeros((8, tok), F32),
        ],
        axis=0,
    ).astype(BF16)
    pick_iota = lax.broadcasted_iota(jnp.int32, (groups * slots, tok), 0)
    picked = (pick_iota == key).astype(F32).astype(BF16)
    wide_iota = lax.broadcasted_iota(jnp.int32, (groups * LANES, tok), 0)
    wide = (wide_iota == step_of * LANES + slot).astype(F32).astype(BF16)
    told = lax.dot_general(
        facts, wide, (((1,), (1,)), ((), ())), preferred_element_type=F32
    ).astype(BF16)
    meta[0] = told[:, :LANES]
    for i in range(1, groups):
        pack_meta[i] = told[:, i * LANES : (i + 1) * LANES]
    for cols in chunks(width, 256):
        block = split_rows(dot(picked, normed[:, cols]), groups)
        blk[0, :, cols] = block[0]
        pack[1:, :, cols] = block[1:]

    def s1_copy(i):
        return pltpu.make_async_remote_copy(
            src_ref=pack.at[i], dst_ref=blk.at[i], send_sem=s1_send.at[i], recv_sem=s1_recv.at[i],
            device_id=(far(i),), device_id_type=MESH,
        )

    def meta_copy(i):
        return pltpu.make_async_remote_copy(
            src_ref=pack_meta.at[i], dst_ref=meta.at[i], send_sem=m_send.at[i], recv_sem=m_recv.at[i],
            device_id=(far(i),), device_id_type=MESH,
        )

    def s2_copy(i, k):
        peer = xor(member, k, MEMBERS)
        return pltpu.make_async_remote_copy(
            src_ref=sel.at[i, peer], dst_ref=rows.at[i, member],
            send_sem=s2_send.at[i, k], recv_sem=s2_recv.at[i, k],
            device_id=(near(k),), device_id_type=MESH,
        )

    def r2_copy(i, k):
        peer = xor(member, k, MEMBERS)
        return pltpu.make_async_remote_copy(
            src_ref=outs.at[i, peer], dst_ref=obuf.at[i, member],
            send_sem=r2_send.at[i, k], recv_sem=r2_recv.at[i, k],
            device_id=(near(k),), device_id_type=MESH,
        )

    def r1_copy(i):
        return pltpu.make_async_remote_copy(
            src_ref=comb.at[i], dst_ref=back.at[i], send_sem=r1_send.at[i], recv_sem=r1_recv.at[i],
            device_id=(far(i),), device_id_type=MESH,
        )

    pl.semaphore_wait(barrier, MEMBERS - 1 + groups - 1)

    sends = sends_in_order(groups)

    @pl.loop(0, groups - 1)
    def _(t):
        i = entry(sends, t)
        meta_copy(i).start()
        s1_copy(i).start()

    place_iota = lax.broadcasted_iota(jnp.int32, (cap, LANES), 0).astype(F32) + 1.0

    def one_hots(i):
        info = meta[i].astype(F32)
        return info, [(place_iota == info[m : m + 1, :]) for m in range(MEMBERS)]

    def select(i):
        @pl.when(i > 0)
        def _():
            meta_copy(i).wait_recv()
            s1_copy(i).wait_recv()

        _, hots = one_hots(i)
        pick = jnp.concatenate([h.astype(F32) for h in hots], axis=0).astype(BF16)[:, :slots]
        for cols in chunks(width, 512):
            sel[i, :, :, cols] = split_rows(dot(pick, blk[i, :, cols]), MEMBERS)
        for k in (2, 3, 1):
            s2_copy(i, k).start()
        rows[i, member] = sel[i, member]

    def ffn(i):
        @pl.when(i == 0)
        def _():
            for load in loads:
                load.wait()

        for k in range(1, MEMBERS):
            s2_copy(i, k).wait_recv()
        x = merge_rows(rows[i])
        for cols in chunks(ff, 256):
            gate_part = dot(x, wg[:, cols])
            up_part = dot(x, wu[:, cols])
            hidden[:, cols] = (gate_part / (1.0 + jnp.exp(-gate_part)) * up_part).astype(BF16)
        h = hidden[...]
        for cols in chunks(width, 256):
            outs[i, :, :, cols] = split_rows(dot(h, wd[:, cols]), MEMBERS)
        for k in (2, 3, 1):
            r2_copy(i, k).start()
        obuf[i, member] = outs[i, member]

    def mix(i):
        for k in range(1, MEMBERS):
            r2_copy(i, k).wait_recv()
        info, hots = one_hots(i)

        def weights(row):
            parts = [jnp.where(hots[m], info[row + m : row + m + 1, :], 0.0) for m in range(MEMBERS)]
            return jnp.concatenate(parts, axis=0).T[:slots].astype(BF16)

        high, low = weights(8), weights(16)

        def mixed(cols):
            values = merge_rows(obuf[i, :, :, cols])
            return (dot(high, values) + dot(low, values)).astype(BF16)

        @pl.when(i == 0)
        def _():
            for cols in chunks(width, 512):
                back[0, :, cols] = mixed(cols)

        @pl.when(i > 0)
        def _():
            for cols in chunks(width, 512):
                comb[i, :, cols] = mixed(cols)
            r1_copy(i).start()

    order = steps_in_order(groups)

    @pl.loop(0, groups + MIX_LAG)
    def _(t):
        @pl.when(t < groups)
        def _():
            select(entry(order, t))

        @pl.when((t >= FFN_LAG) & (t < groups + FFN_LAG))
        def _():
            ffn(entry(order, t - FFN_LAG))

        @pl.when(t >= MIX_LAG)
        def _():
            mix(entry(order, t - MIX_LAG))

    key_column = jnp.broadcast_to(key.astype(F32), (LANES, tok)).T[:, 0:1].astype(jnp.int32)
    spread = (
        lax.broadcasted_iota(jnp.int32, (tok, groups * slots), 1) == key_column
    ).astype(F32).astype(BF16)

    @pl.loop(1, groups)
    def _(i):
        r1_copy(i).wait_recv()

    for cols in chunks(width, 256):
        out_ref[:, cols] = dot(spread, merge_rows(back[:, :, cols])).astype(BF16)

    @pl.loop(0, groups)
    def _(i):
        @pl.when(i > 0)
        def _():
            meta_copy(i).wait_send()
            s1_copy(i).wait_send()
            r1_copy(i).wait_send()

        for k in range(1, MEMBERS):
            s2_copy(i, k).wait_send()
            r2_copy(i, k).wait_send()


def shards(tokens, norm_gain, expert_ids, gates, w_gate, w_up, w_down):
    tok, width = tokens.shape
    ff = w_gate.shape[2]
    experts = lax.axis_size("ep")
    groups = experts // MEMBERS
    cap = 2 * ((2 * tok + experts - 1) // experts)
    slots = 2 * cap
    vmem = pl.BlockSpec(memory_space=pltpu.VMEM)
    hbm = pl.BlockSpec(memory_space=pl.ANY)
    dma = pltpu.SemaphoreType.DMA
    by_group = pltpu.VMEM((groups, slots, width), BF16)
    by_member = pltpu.VMEM((groups, MEMBERS, cap, width), BF16)
    facts = pltpu.VMEM((groups, 32, LANES), BF16)
    return pl.pallas_call(
        functools.partial(kernel, groups, cap),
        out_shape=jax.ShapeDtypeStruct((tok, width), BF16),
        in_specs=[vmem] * 4 + [hbm] * 3,
        out_specs=vmem,
        scratch_shapes=[
            pltpu.VMEM((width, ff), BF16), pltpu.VMEM((width, ff), BF16), pltpu.VMEM((ff, width), BF16),
            pltpu.VMEM((tok, width), BF16),
            by_group, facts, by_group, facts, by_member, by_member,
            pltpu.VMEM((MEMBERS * cap, ff), BF16),
            by_member, by_member, by_group, by_group,
            dma((3,)), dma((groups,)), dma((groups,)), dma((groups,)), dma((groups,)),
            dma((groups, MEMBERS)), dma((groups, MEMBERS)), dma((groups, MEMBERS)), dma((groups, MEMBERS)),
            dma((groups,)), dma((groups,)),
        ],
        compiler_params=pltpu.CompilerParams(
            collective_id=0, has_side_effects=True, vmem_limit_bytes=58 * 1024 * 1024
        ),
    )(expert_ids.T, gates.T, tokens, norm_gain.reshape(1, width), w_gate, w_up, w_down)


def solution(mesh):
    return jax.shard_map(
        shards,
        mesh=mesh,
        in_specs=(
            P("ep", None),
            P(),
            P("ep", None),
            P("ep", None),
            P("ep", None, None),
            P("ep", None, None),
            P("ep", None, None),
        ),
        out_specs=P("ep", None),
        check_vma=False,
    )
```

profile of v0, /device:TPU:0, one launch (start us, length us, event | category | flops | bytes accessed | tf_op | source)
XLA Modules:
  0.0 119.7 jit_solution(3313050021503370720)
XLA Ops:
  0.0 117.4 %shard_map.73 = bf16[256,2048]{1,0:T(8,128)(2,1)} custom-call(s32[2,256]{1,0:T(2,128)} %bitcast.4, f32[2,256]{1,0:T(2,128)} %bitcast.5, bf16[256,2048]{1,0:T(8,128)(2,1)} %tokens_ref.1, f32[1,2048]{1,0:T(1,128)} %bitcast.3, bf16[1,2048,1024]{2,1,0:T(8,128)(2,1)} %wg_hbm.1, bf16[1,2048,1024]{2,1,0:T(8,128)(2,1)} %wu_hbm.1, bf16[1,1024,2048]{2,1,0:T(8,128)(2,1)} %wd_hbm.1), custom_call_target="tpu_custom_call" | custom-call | tf_op jit(solution)/shard_map/pallas_call | solution.py:322
  117.4 2.3 %copy.9 = bf16[256,2048]{1,0:T(8,128)(2,1)} copy(bf16[256,2048]{1,0:T(8,128)(2,1)} %shard_map.73) | data formatting | bytes 2097152
where the time goes:
time: 121 us; the launch traced here: 120 us
  Pallas kernels  117 us (97%)
  local copies, waits for them, and re-layouts  2.3 us (2%)
    pallas_call x1, Pallas kernels, shards(): pl.pallas_call(functools.partial(kernel, groups, cap), out_shape=jax.Shap...  117 us

commit v1 on v0

--- a/solution.py
+++ b/solution.py
@@ -9,8 +9,6 @@
 
 EPS = 1e-06
 MEMBERS = 4
-FFN_LAG = 1
-MIX_LAG = 2
 LANES = 128
 MESH = pl.DeviceIdType.MESH
 F32 = jnp.float32
@@ -25,18 +23,34 @@
     return total
 
 
-def steps_in_order(groups):
-    upper = list(range(groups // 2, groups))
-    lower = list(range(1, groups // 2))
-    middle = []
+def bits(i):
+    return bin(i).count("1")
+
+
+def select_order(groups):
+    half = groups // 2
+    upper = sorted(range(half, groups), key=lambda i: (bits(i), -i))
+    lower = sorted(range(1, half), key=lambda i: (bits(i), i))
+    order, lower = [0, *lower[:2]], lower[2:]
     while upper or lower:
-        middle += lower[:1] + upper[:2]
-        lower, upper = lower[1:], upper[2:]
-    return [0, *middle]
-
-
-def sends_in_order(groups):
-    return steps_in_order(groups)[1:]
+        order += upper[:2] + lower[:1]
+        upper, lower = upper[2:], lower[1:]
+    return order
+
+
+def output_order(groups):
+    order = select_order(groups)
+    half = groups // 2
+    return [i for i in order if i >= half] + [i for i in order if 0 < i < half] + [0]
+
+
+def output_lag(groups):
+    first, second = select_order(groups), output_order(groups)
+    return 1 + max(first.index(i) - second.index(i) for i in range(groups))
+
+
+def send_order(groups, distance):
+    return [i for i in select_order(groups) if bits(i) == distance]
 
 
 def entry(table, t):
@@ -66,9 +80,9 @@
 
 def kernel(
     groups, cap,
-    ids_ref, gates_ref, tokens_ref, gain_ref, wg_hbm, wu_hbm, wd_hbm, out_ref,
-    wg, wu, wd, normed, pack, pack_meta, blk, meta, sel, rows, hidden, outs, obuf, comb, back,
-    w_sem, s1_send, s1_recv, m_send, m_recv, s2_send, s2_recv, r2_send, r2_recv, r1_send, r1_recv,
+    ids_hbm, gates_hbm, tokens_hbm, gain_hbm, wg_hbm, wu_hbm, wd_hbm, out_ref,
+    ids_ref, gates_ref, tokens_ref, gain_ref, wg, wu, wd, normed, pack, pack_meta, blk, meta, sel, rows, hidden, outs, obuf, comb, back,
+    in_sem, w_sem, near_sem, s1_send, s1_recv, m_send, m_recv, s2_send, s2_recv, r2_send, r2_recv, r1_send, r1_recv,
 ):
     tok, width = tokens_ref.shape
     ff = wg.shape[1]
@@ -77,32 +91,38 @@
     me = lax.axis_index("ep")
     group, member = me // MEMBERS, me % MEMBERS
 
+    def far(i):
+        return xor(group, i, groups) * MEMBERS + member
+
+    def near(k):
+        return group * MEMBERS + xor(member, k, MEMBERS)
+
+    distances = bits(groups - 1)
+    barrier = pltpu.get_barrier_semaphore()
+    for k in range(1, MEMBERS):
+        pl.semaphore_signal(barrier, inc=1, device_id=(near(k),), device_id_type=MESH)
+    for b in range(distances):
+        pl.semaphore_signal(barrier, inc=1, device_id=(far(2**b),), device_id_type=MESH)
+
+    block = min(tok, 64)
+    small = [
+        pltpu.make_async_copy(src, dst, in_sem.at[k])
+        for k, (src, dst) in enumerate(((ids_hbm, ids_ref), (gates_hbm, gates_ref), (gain_hbm, gain_ref)))
+    ]
+    token_loads = [
+        pltpu.make_async_copy(
+            tokens_hbm.at[pl.ds(r, block)], tokens_ref.at[pl.ds(r, block)], in_sem.at[3 + r // block]
+        )
+        for r in range(0, tok, block)
+    ]
     loads = [
         pltpu.make_async_copy(src.at[0], dst, w_sem.at[k])
         for k, (src, dst) in enumerate(((wg_hbm, wg), (wu_hbm, wu), (wd_hbm, wd)))
     ]
-    for load in loads:
+    for load in small + token_loads + loads:
         load.start()
-
-    def far(i):
-        return xor(group, i, groups) * MEMBERS + member
-
-    def near(k):
-        return group * MEMBERS + xor(member, k, MEMBERS)
-
-    barrier = pltpu.get_barrier_semaphore()
-    for k in range(1, MEMBERS):
-        pl.semaphore_signal(barrier, inc=1, device_id=(near(k),), device_id_type=MESH)
-
-    @pl.loop(1, groups)
-    def _(i):
-        pl.semaphore_signal(barrier, inc=1, device_id=(far(i),), device_id_type=MESH)
-
-    for r in range(0, tok, 64):
-        part = pl.ds(r, min(64, tok))
-        floats = tokens_ref[part, :].astype(F32)
-        inverse = lax.rsqrt(jnp.mean(floats * floats, axis=-1, keepdims=True) + EPS)
-        normed[part, :] = (floats * inverse * gain_ref[...]).astype(BF16)
+    for load in small:
+        load.wait()
 
     ids = ids_ref[...]
     first, second = ids[0:1, :], ids[1:2, :]
@@ -150,10 +170,17 @@
     meta[0] = told[:, :LANES]
     for i in range(1, groups):
         pack_meta[i] = told[:, i * LANES : (i + 1) * LANES]
+    for r in range(0, tok, block):
+        token_loads[r // block].wait()
+        part = pl.ds(r, block)
+        floats = tokens_ref[part, :].astype(F32)
+        inverse = lax.rsqrt(jnp.mean(floats * floats, axis=-1, keepdims=True) + EPS)
+        normed[part, :] = (floats * inverse * gain_ref[...]).astype(BF16)
+
     for cols in chunks(width, 256):
-        block = split_rows(dot(picked, normed[:, cols]), groups)
-        blk[0, :, cols] = block[0]
-        pack[1:, :, cols] = block[1:]
+        packed = split_rows(dot(picked, normed[:, cols]), groups)
+        blk[0, :, cols] = packed[0]
+        pack[1:, :, cols] = packed[1:]
 
     def s1_copy(i):
         return pltpu.make_async_remote_copy(
@@ -189,15 +216,21 @@
             device_id=(far(i),), device_id_type=MESH,
         )
 
-    pl.semaphore_wait(barrier, MEMBERS - 1 + groups - 1)
-
-    sends = sends_in_order(groups)
-
-    @pl.loop(0, groups - 1)
-    def _(t):
-        i = entry(sends, t)
-        meta_copy(i).start()
-        s1_copy(i).start()
+    def send(distance):
+        if distance == 1:
+            pl.semaphore_wait(barrier, MEMBERS - 1 + distances)
+        else:
+            pl.semaphore_wait(near_sem.at[distance], distances)
+        if distance < distances:
+            for b in range(distances):
+                pl.semaphore_signal(
+                    near_sem.at[distance + 1], inc=1, device_id=(far(2**b),), device_id_type=MESH
+                )
+        for i in send_order(groups, distance):
+            meta_copy(i).start()
+            s1_copy(i).start()
+
+    send(1)
 
     place_iota = lax.broadcasted_iota(jnp.int32, (cap, LANES), 0).astype(F32) + 1.0
 
@@ -219,8 +252,8 @@
             s2_copy(i, k).start()
         rows[i, member] = sel[i, member]
 
-    def ffn(i):
-        @pl.when(i == 0)
+    def ffn(i, is_first):
+        @pl.when(is_first)
         def _():
             for load in loads:
                 load.wait()
@@ -265,21 +298,26 @@
                 comb[i, :, cols] = mixed(cols)
             r1_copy(i).start()
 
-    order = steps_in_order(groups)
-
-    @pl.loop(0, groups + MIX_LAG)
+    first, second, lag = select_order(groups), output_order(groups), output_lag(groups)
+
+    @pl.loop(0, groups + lag + 1)
     def _(t):
         @pl.when(t < groups)
         def _():
-            select(entry(order, t))
-
-        @pl.when((t >= FFN_LAG) & (t < groups + FFN_LAG))
-        def _():
-            ffn(entry(order, t - FFN_LAG))
-
-        @pl.when(t >= MIX_LAG)
-        def _():
-            mix(entry(order, t - MIX_LAG))
+            select(entry(first, t))
+
+        for d in range(2, distances + 1):
+            @pl.when(t == d - 2)
+            def _():
+                send(d)
+
+        @pl.when((t >= lag) & (t < groups + lag))
+        def _():
+            ffn(entry(second, t - lag), t == lag)
+
+        @pl.when(t >= lag + 1)
+        def _():
+            mix(entry(second, t - lag - 1))
 
     key_column = jnp.broadcast_to(key.astype(F32), (LANES, tok)).T[:, 0:1].astype(jnp.int32)
     spread = (
@@ -322,15 +360,18 @@
     return pl.pallas_call(
         functools.partial(kernel, groups, cap),
         out_shape=jax.ShapeDtypeStruct((tok, width), BF16),
-        in_specs=[vmem] * 4 + [hbm] * 3,
+        in_specs=[hbm] * 7,
         out_specs=vmem,
         scratch_shapes=[
+            pltpu.VMEM((2, tok), jnp.int32), pltpu.VMEM((2, tok), F32),
+            pltpu.VMEM((tok, width), BF16), pltpu.VMEM((1, width), F32),
             pltpu.VMEM((width, ff), BF16), pltpu.VMEM((width, ff), BF16), pltpu.VMEM((ff, width), BF16),
             pltpu.VMEM((tok, width), BF16),
             by_group, facts, by_group, facts, by_member, by_member,
             pltpu.VMEM((MEMBERS * cap, ff), BF16),
             by_member, by_member, by_group, by_group,
-            dma((3,)), dma((groups,)), dma((groups,)), dma((groups,)), dma((groups,)),
+            dma((3 + tok // min(tok, 64),)), dma((3,)), pltpu.SemaphoreType.REGULAR((groups.bit_length(),)),
+            dma((groups,)), dma((groups,)), dma((groups,)), dma((groups,)),
             dma((groups, MEMBERS)), dma((groups, MEMBERS)), dma((groups, MEMBERS)), dma((groups, MEMBERS)),
             dma((groups,)), dma((groups,)),
         ],

time: 121 us -> 113 us (0.934); the launches traced: 120 us -> 113 us
  Pallas kernels: 117 us -> 111 us
    pallas_call x1, Pallas kernels: 117 us -> 111 us  [shards(): pl.pallas_call(functools.partial(kernel, groups, cap), out_shape=jax.Shap...]
where the time goes in v1:
time: 113 us
  Pallas kernels  111 us (98%)
  local copies, waits for them, and re-layouts  2.3 us (2%)
    pallas_call x1, Pallas kernels, shards(): pl.pallas_call(functools.partial(kernel, groups, cap), out_shape=jax.Shap...  111 us
    unnamed x1, local copies, waits for them, and re-layouts  2.3 us

profile of v1, /device:TPU:0, one launch (start us, length us, event | category | flops | bytes accessed | tf_op | source)
XLA Modules:
  0.0 113.0 jit_solution(11231045463741953721)
XLA Ops:
  0.0 110.7 %shard_map.73 = bf16[256,2048]{1,0:T(8,128)(2,1)} custom-call(s32[2,256]{1,0:T(2,128)} %bitcast.4, f32[2,256]{1,0:T(2,128)} %bitcast.5, bf16[256,2048]{1,0:T(8,128)(2,1)} %tokens_hbm.1, f32[1,2048]{1,0:T(1,128)} %bitcast.3, bf16[1,2048,1024]{2,1,0:T(8,128)(2,1)} %wg_hbm.1, bf16[1,2048,1024]{2,1,0:T(8,128)(2,1)} %wu_hbm.1, bf16[1,1024,2048]{2,1,0:T(8,128)(2,1)} %wd_hbm.1), custom_call_target="tpu_custom_call" | custom-call | tf_op jit(solution)/shard_map/pallas_call | solution.py:360
  110.7 2.3 %copy.9 = bf16[256,2048]{1,0:T(8,128)(2,1)} copy(bf16[256,2048]{1,0:T(8,128)(2,1)} %shard_map.73) | data formatting | bytes 2097152

commit v2 on v1

--- a/solution.py
+++ b/solution.py
@@ -27,34 +27,70 @@
     return bin(i).count("1")
 
 
-def select_order(groups):
+def halves(groups):
     half = groups // 2
     upper = sorted(range(half, groups), key=lambda i: (bits(i), -i))
     lower = sorted(range(1, half), key=lambda i: (bits(i), i))
-    order, lower = [0, *lower[:2]], lower[2:]
+    return upper, lower
+
+
+def send_order(groups, distance):
+    upper, lower = ([i for i in items if bits(i) == distance] for items in halves(groups))
+    if distance == 1:
+        return lower + upper
+    order = []
     while upper or lower:
-        order += upper[:2] + lower[:1]
-        upper, lower = upper[2:], lower[1:]
+        order += upper[:1] + lower[:1]
+        upper, lower = upper[1:], lower[1:]
     return order
 
 
-def output_order(groups):
-    order = select_order(groups)
-    half = groups // 2
-    return [i for i in order if i >= half] + [i for i in order if 0 < i < half] + [0]
-
-
-def output_lag(groups):
-    first, second = select_order(groups), output_order(groups)
-    return 1 + max(first.index(i) - second.index(i) for i in range(groups))
-
-
-def send_order(groups, distance):
-    return [i for i in select_order(groups) if bits(i) == distance]
+def plan(groups):
+    upper, lower = halves(groups)
+    near = [i for i in lower if bits(i) == 1]
+    rest = [i for i in lower if bits(i) > 1]
+    steps, waiting = [], []
+
+    def select(*items):
+        steps.extend((0, i) for i in items)
+
+    def mix(keep):
+        while len(waiting) > keep:
+            steps.append((1, waiting.pop(0)))
+
+    def output(*items):
+        steps.extend((2, i) for i in items)
+        waiting.extend(items)
+
+    select(0, *near, upper[0])
+    output(near[0])
+    select(upper[1])
+    output(upper[0], *near[1:])
+    for before, i in zip(upper[1:], upper[2:]):
+        select(i)
+        mix(1)
+        output(before)
+    mix(1)
+    select(*rest)
+    output(upper[-1])
+    mix(1)
+    output(*rest, 0)
+    mix(0)
+
+    rows, last = [], 2
+    for kind, item in steps:
+        if kind <= last:
+            rows.append([-1, -1, -1])
+        rows[-1][kind] = item
+        last = kind
+    return [list(column) for column in zip(*rows)]
+
+
+PARTS = 2
 
 
 def entry(table, t):
-    return sum(jnp.where(t == k, value, 0) for k, value in enumerate(table))
+    return sum(jnp.where(t == k, value, 0) for k, value in enumerate(table) if value)
 
 
 def merge_rows(block):
@@ -81,6 +117,7 @@
 def kernel(
     groups, cap,
     ids_hbm, gates_hbm, tokens_hbm, gain_hbm, wg_hbm, wu_hbm, wd_hbm, out_ref,
+    spread_ref,
     ids_ref, gates_ref, tokens_ref, gain_ref, wg, wu, wd, normed, pack, pack_meta, blk, meta, sel, rows, hidden, outs, obuf, comb, back,
     in_sem, w_sem, near_sem, s1_send, s1_recv, m_send, m_recv, s2_send, s2_recv, r2_send, r2_recv, r1_send, r1_recv,
 ):
@@ -172,49 +209,55 @@
         pack_meta[i] = told[:, i * LANES : (i + 1) * LANES]
     for r in range(0, tok, block):
         token_loads[r // block].wait()
-        part = pl.ds(r, block)
-        floats = tokens_ref[part, :].astype(F32)
+        lines = pl.ds(r, block)
+        floats = tokens_ref[lines, :].astype(F32)
         inverse = lax.rsqrt(jnp.mean(floats * floats, axis=-1, keepdims=True) + EPS)
-        normed[part, :] = (floats * inverse * gain_ref[...]).astype(BF16)
-
-    for cols in chunks(width, 256):
-        packed = split_rows(dot(picked, normed[:, cols]), groups)
-        blk[0, :, cols] = packed[0]
-        pack[1:, :, cols] = packed[1:]
-
-    def s1_copy(i):
+        normed[lines, :] = (floats * inverse * gain_ref[...]).astype(BF16)
+
+    part = width // PARTS
+    for h in range(PARTS):
+        for cols in chunks(part, 256):
+            source = slice(h * part + cols.start, h * part + cols.stop)
+            packed = split_rows(dot(picked, normed[:, source]), groups)
+            blk[0, h, :, cols] = packed[0]
+            pack[1:, h, :, cols] = packed[1:]
+
+    def s1_copy(i, h):
         return pltpu.make_async_remote_copy(
-            src_ref=pack.at[i], dst_ref=blk.at[i], send_sem=s1_send.at[i], recv_sem=s1_recv.at[i],
+            src_ref=pack.at[i, h], dst_ref=blk.at[i, h], send_sem=s1_send.at[0], recv_sem=s1_recv.at[i, h],
             device_id=(far(i),), device_id_type=MESH,
         )
 
     def meta_copy(i):
         return pltpu.make_async_remote_copy(
-            src_ref=pack_meta.at[i], dst_ref=meta.at[i], send_sem=m_send.at[i], recv_sem=m_recv.at[i],
+            src_ref=pack_meta.at[i], dst_ref=meta.at[i], send_sem=m_send.at[0], recv_sem=m_recv.at[i],
             device_id=(far(i),), device_id_type=MESH,
         )
 
-    def s2_copy(i, k):
+    def s2_copy(i, h, k):
         peer = xor(member, k, MEMBERS)
         return pltpu.make_async_remote_copy(
-            src_ref=sel.at[i, peer], dst_ref=rows.at[i, member],
-            send_sem=s2_send.at[i, k], recv_sem=s2_recv.at[i, k],
+            src_ref=sel.at[i, h, peer], dst_ref=rows.at[i, h, member],
+            send_sem=s2_send.at[0], recv_sem=s2_recv.at[i],
             device_id=(near(k),), device_id_type=MESH,
         )
 
-    def r2_copy(i, k):
+    def r2_copy(i, h, k):
         peer = xor(member, k, MEMBERS)
         return pltpu.make_async_remote_copy(
-            src_ref=outs.at[i, peer], dst_ref=obuf.at[i, member],
-            send_sem=r2_send.at[i, k], recv_sem=r2_recv.at[i, k],
+            src_ref=outs.at[i, h, peer], dst_ref=obuf.at[i, h, member],
+            send_sem=r2_send.at[0], recv_sem=r2_recv.at[i, h],
             device_id=(near(k),), device_id_type=MESH,
         )
 
-    def r1_copy(i):
+    def r1_copy(i, h):
         return pltpu.make_async_remote_copy(
-            src_ref=comb.at[i], dst_ref=back.at[i], send_sem=r1_send.at[i], recv_sem=r1_recv.at[i],
+            src_ref=comb.at[i, h], dst_ref=back.at[i, h], send_sem=r1_send.at[0], recv_sem=r1_recv.at[0],
             device_id=(far(i),), device_id_type=MESH,
         )
+
+    def landed(ref, sem):
+        pltpu.make_async_copy(ref, ref, sem).wait()
 
     def send(distance):
         if distance == 1:
@@ -228,7 +271,8 @@
                 )
         for i in send_order(groups, distance):
             meta_copy(i).start()
-            s1_copy(i).start()
+            for h in range(PARTS):
+                s1_copy(i, h).start()
 
     send(1)
 
@@ -242,15 +286,19 @@
         @pl.when(i > 0)
         def _():
             meta_copy(i).wait_recv()
-            s1_copy(i).wait_recv()
 
         _, hots = one_hots(i)
         pick = jnp.concatenate([h.astype(F32) for h in hots], axis=0).astype(BF16)[:, :slots]
-        for cols in chunks(width, 512):
-            sel[i, :, :, cols] = split_rows(dot(pick, blk[i, :, cols]), MEMBERS)
-        for k in (2, 3, 1):
-            s2_copy(i, k).start()
-        rows[i, member] = sel[i, member]
+        for h in range(PARTS):
+            @pl.when(i > 0)
+            def _():
+                s1_copy(i, h).wait_recv()
+
+            for cols in chunks(part, 512):
+                sel[i, h, :, :, cols] = split_rows(dot(pick, blk[i, h, :, cols]), MEMBERS)
+            for k in (2, 3, 1):
+                s2_copy(i, h, k).start()
+            rows[i, h, member] = sel[i, h, member]
 
     def ffn(i, is_first):
         @pl.when(is_first)
@@ -258,23 +306,22 @@
             for load in loads:
                 load.wait()
 
-        for k in range(1, MEMBERS):
-            s2_copy(i, k).wait_recv()
-        x = merge_rows(rows[i])
+        landed(rows.at[i, :, 1:], s2_recv.at[i])
+        xs = [merge_rows(rows[i, h]) for h in range(PARTS)]
         for cols in chunks(ff, 256):
-            gate_part = dot(x, wg[:, cols])
-            up_part = dot(x, wu[:, cols])
+            gate_part = sum(dot(x, wg[h * part : (h + 1) * part, cols]) for h, x in enumerate(xs))
+            up_part = sum(dot(x, wu[h * part : (h + 1) * part, cols]) for h, x in enumerate(xs))
             hidden[:, cols] = (gate_part / (1.0 + jnp.exp(-gate_part)) * up_part).astype(BF16)
-        h = hidden[...]
-        for cols in chunks(width, 256):
-            outs[i, :, :, cols] = split_rows(dot(h, wd[:, cols]), MEMBERS)
-        for k in (2, 3, 1):
-            r2_copy(i, k).start()
-        obuf[i, member] = outs[i, member]
+        hid = hidden[...]
+        for h in range(PARTS):
+            for cols in chunks(part, 256):
+                source = slice(h * part + cols.start, h * part + cols.stop)
+                outs[i, h, :, :, cols] = split_rows(dot(hid, wd[:, source]), MEMBERS)
+            for k in (2, 3, 1):
+                r2_copy(i, h, k).start()
+            obuf[i, h, member] = outs[i, h, member]
 
     def mix(i):
-        for k in range(1, MEMBERS):
-            r2_copy(i, k).wait_recv()
         info, hots = one_hots(i)
 
         def weights(row):
@@ -283,65 +330,63 @@
 
         high, low = weights(8), weights(16)
 
-        def mixed(cols):
-            values = merge_rows(obuf[i, :, :, cols])
+        def mixed(h, cols):
+            values = merge_rows(obuf[i, h, :, :, cols])
             return (dot(high, values) + dot(low, values)).astype(BF16)
 
-        @pl.when(i == 0)
+        for h in range(PARTS):
+            landed(obuf.at[i, h, 1:], r2_recv.at[i, h])
+
+            @pl.when(i == 0)
+            def _():
+                for cols in chunks(part, 512):
+                    back[0, h, :, cols] = mixed(h, cols)
+
+            @pl.when(i > 0)
+            def _():
+                for cols in chunks(part, 512):
+                    comb[i, h, :, cols] = mixed(h, cols)
+                r1_copy(i, h).start()
+
+    key_column = jnp.broadcast_to(key.astype(F32), (LANES, tok)).T[:, 0:1].astype(jnp.int32)
+    spread_ref[...] = (
+        lax.broadcasted_iota(jnp.int32, (tok, groups * slots), 1) == key_column
+    ).astype(F32).astype(BF16)
+
+    selects, mixes, outputs = plan(groups)
+    first_output = next(t for t, i in enumerate(outputs) if i >= 0)
+
+    @pl.loop(0, len(selects))
+    def _(t):
+        to_select, to_mix, to_output = entry(selects, t), entry(mixes, t), entry(outputs, t)
+
+        @pl.when(to_select >= 0)
         def _():
-            for cols in chunks(width, 512):
-                back[0, :, cols] = mixed(cols)
-
-        @pl.when(i > 0)
-        def _():
-            for cols in chunks(width, 512):
-                comb[i, :, cols] = mixed(cols)
-            r1_copy(i).start()
-
-    first, second, lag = select_order(groups), output_order(groups), output_lag(groups)
-
-    @pl.loop(0, groups + lag + 1)
-    def _(t):
-        @pl.when(t < groups)
-        def _():
-            select(entry(first, t))
+            select(to_select)
 
         for d in range(2, distances + 1):
             @pl.when(t == d - 2)
             def _():
                 send(d)
 
-        @pl.when((t >= lag) & (t < groups + lag))
+        @pl.when(to_mix >= 0)
         def _():
-            ffn(entry(second, t - lag), t == lag)
-
-        @pl.when(t >= lag + 1)
+            mix(to_mix)
+
+        @pl.when(to_output >= 0)
         def _():
-            mix(entry(second, t - lag - 1))
-
-    key_column = jnp.broadcast_to(key.astype(F32), (LANES, tok)).T[:, 0:1].astype(jnp.int32)
-    spread = (
-        lax.broadcasted_iota(jnp.int32, (tok, groups * slots), 1) == key_column
-    ).astype(F32).astype(BF16)
-
-    @pl.loop(1, groups)
-    def _(i):
-        r1_copy(i).wait_recv()
-
-    for cols in chunks(width, 256):
-        out_ref[:, cols] = dot(spread, merge_rows(back[:, :, cols])).astype(BF16)
-
-    @pl.loop(0, groups)
-    def _(i):
-        @pl.when(i > 0)
-        def _():
-            meta_copy(i).wait_send()
-            s1_copy(i).wait_send()
-            r1_copy(i).wait_send()
-
-        for k in range(1, MEMBERS):
-            s2_copy(i, k).wait_send()
-            r2_copy(i, k).wait_send()
+            ffn(to_output, t == first_output)
+
+    landed(pack.at[1:], s1_send.at[0])
+    landed(pack_meta.at[1:], m_send.at[0])
+    landed(sel.at[:, :, 1:], s2_send.at[0])
+    landed(outs.at[:, :, 1:], r2_send.at[0])
+    landed(comb.at[1:], r1_send.at[0])
+    landed(back.at[1:], r1_recv.at[0])
+    for h in range(PARTS):
+        for cols in chunks(part, 512):
+            target = pl.ds(h * part + cols.start, cols.stop - cols.start)
+            out_ref[:, target] = dot(spread_ref[...], merge_rows(back[:, h, :, cols])).astype(BF16)
 
 
 def shards(tokens, norm_gain, expert_ids, gates, w_gate, w_up, w_down):
@@ -351,18 +396,18 @@
     groups = experts // MEMBERS
     cap = 2 * ((2 * tok + experts - 1) // experts)
     slots = 2 * cap
-    vmem = pl.BlockSpec(memory_space=pltpu.VMEM)
-    hbm = pl.BlockSpec(memory_space=pl.ANY)
+    hbm = pl.BlockSpec(memory_space=pltpu.HBM)
     dma = pltpu.SemaphoreType.DMA
-    by_group = pltpu.VMEM((groups, slots, width), BF16)
-    by_member = pltpu.VMEM((groups, MEMBERS, cap, width), BF16)
+    by_group = pltpu.VMEM((groups, PARTS, slots, width // PARTS), BF16)
+    by_member = pltpu.VMEM((groups, PARTS, MEMBERS, cap, width // PARTS), BF16)
     facts = pltpu.VMEM((groups, 32, LANES), BF16)
     return pl.pallas_call(
         functools.partial(kernel, groups, cap),
         out_shape=jax.ShapeDtypeStruct((tok, width), BF16),
         in_specs=[hbm] * 7,
-        out_specs=vmem,
+        out_specs=pl.BlockSpec(memory_space=pltpu.VMEM),
         scratch_shapes=[
+            pltpu.VMEM((tok, groups * slots), BF16),
             pltpu.VMEM((2, tok), jnp.int32), pltpu.VMEM((2, tok), F32),
             pltpu.VMEM((tok, width), BF16), pltpu.VMEM((1, width), F32),
             pltpu.VMEM((width, ff), BF16), pltpu.VMEM((width, ff), BF16), pltpu.VMEM((ff, width), BF16),
@@ -371,14 +416,13 @@
             pltpu.VMEM((MEMBERS * cap, ff), BF16),
             by_member, by_member, by_group, by_group,
             dma((3 + tok // min(tok, 64),)), dma((3,)), pltpu.SemaphoreType.REGULAR((groups.bit_length(),)),
-            dma((groups,)), dma((groups,)), dma((groups,)), dma((groups,)),
-            dma((groups, MEMBERS)), dma((groups, MEMBERS)), dma((groups, MEMBERS)), dma((groups, MEMBERS)),
-            dma((groups,)), dma((groups,)),
+            dma((1,)), dma((groups, PARTS)), dma((1,)), dma((groups,)),
+            dma((1,)), dma((groups,)), dma((1,)), dma((groups, PARTS)), dma((1,)), dma((1,)),
         ],
         compiler_params=pltpu.CompilerParams(
-            collective_id=0, has_side_effects=True, vmem_limit_bytes=58 * 1024 * 1024
+            collective_id=0, has_side_effects=True, vmem_limit_bytes=50 * 1024 * 1024
         ),
-    )(expert_ids.T, gates.T, tokens, norm_gain.reshape(1, width), w_gate, w_up, w_down)
+    )(*[pltpu.with_memory_space_constraint(a, pltpu.HBM) for a in (expert_ids.T, gates.T, tokens, norm_gain.reshape(1, width), w_gate, w_up, w_down)])
 
 
 def solution(mesh):

time: 113 us -> 106 us (0.938)
  Pallas kernels: 111 us -> 104 us
  local copies, waits for them, and re-layouts: 2.3 us -> 0.97 us
    pallas_call x1, Pallas kernels: 111 us -> 104 us  [shards(): pl.pallas_call(functools.partial(kernel, groups, cap), out_shape=jax.Shap...]
    unnamed x1, local copies, waits for them, and re-layouts: 2.3 us -> 0.97 us
where the time goes in v2:
time: 106 us; the launch traced here: 105 us
  Pallas kernels  104 us (98%)
    pallas_call x1, Pallas kernels, shards(): pl.pallas_call(functools.partial(kernel, groups, cap), out_shape=jax.Shap...  104 us

profile of v2, /device:TPU:0, one launch (start us, length us, event | category | flops | bytes accessed | tf_op | source)
XLA Modules:
  0.0 105.4 jit_solution(11260483727141583111)
XLA Ops:
  0.0 104.4 %shard_map.73 = bf16[256,2048]{1,0:T(8,128)(2,1)S(1)} custom-call(s32[2,256]{1,0:T(2,128)} %bitcast.4, f32[2,256]{1,0:T(2,128)} %bitcast.5, bf16[256,2048]{1,0:T(8,128)(2,1)} %tokens_hbm.1, f32[1,2048]{1,0:T(1,128)} %bitcast.3, bf16[1,2048,1024]{2,1,0:T(8,128)(2,1)} %wg_hbm.1, bf16[1,2048,1024]{2,1,0:T(8,128)(2,1)} %wu_hbm.1, bf16[1,1024,2048]{2,1,0:T(8,128)(2,1)} %wd_hbm.1), custom_call_target="tpu_custom_call" | custom-call | tf_op jit(solution)/shard_map/pallas_call | solution.py:404
  104.4 1.0 copy.9

commit v3 on v2

--- a/solution.py
+++ b/solution.py
@@ -156,7 +156,7 @@
         pltpu.make_async_copy(src.at[0], dst, w_sem.at[k])
         for k, (src, dst) in enumerate(((wg_hbm, wg), (wu_hbm, wu), (wd_hbm, wd)))
     ]
-    for load in small + token_loads + loads:
+    for load in small + token_loads:
         load.start()
     for load in small:
         load.wait()
@@ -207,12 +207,16 @@
     meta[0] = told[:, :LANES]
     for i in range(1, groups):
         pack_meta[i] = told[:, i * LANES : (i + 1) * LANES]
-    for r in range(0, tok, block):
-        token_loads[r // block].wait()
-        lines = pl.ds(r, block)
+    for r in range(0, tok, min(tok, 16)):
+        if r % block == 0:
+            token_loads[r // block].wait()
+        lines = pl.ds(r, min(tok, 16))
         floats = tokens_ref[lines, :].astype(F32)
         inverse = lax.rsqrt(jnp.mean(floats * floats, axis=-1, keepdims=True) + EPS)
         normed[lines, :] = (floats * inverse * gain_ref[...]).astype(BF16)
+
+    for load in loads:
+        load.start()
 
     part = width // PARTS
     for h in range(PARTS):
@@ -348,11 +352,6 @@
                     comb[i, h, :, cols] = mixed(h, cols)
                 r1_copy(i, h).start()
 
-    key_column = jnp.broadcast_to(key.astype(F32), (LANES, tok)).T[:, 0:1].astype(jnp.int32)
-    spread_ref[...] = (
-        lax.broadcasted_iota(jnp.int32, (tok, groups * slots), 1) == key_column
-    ).astype(F32).astype(BF16)
-
     selects, mixes, outputs = plan(groups)
     first_output = next(t for t, i in enumerate(outputs) if i >= 0)
 
@@ -368,6 +367,13 @@
             @pl.when(t == d - 2)
             def _():
                 send(d)
+
+        @pl.when(t == 1)
+        def _():
+            key_column = jnp.broadcast_to(key.astype(F32), (LANES, tok)).T[:, 0:1].astype(jnp.int32)
+            spread_ref[...] = (
+                lax.broadcasted_iota(jnp.int32, (tok, groups * slots), 1) == key_column
+            ).astype(F32).astype(BF16)
 
         @pl.when(to_mix >= 0)
         def _():

time: 106 us -> 104 us (0.981)
  Pallas kernels: 104 us -> 102 us
    pallas_call x1, Pallas kernels: 104 us -> 102 us  [shards(): pl.pallas_call(functools.partial(kernel, groups, cap), out_shape=jax.Shap...]
where the time goes in v3:
time: 104 us; the launch traced here: 103 us
  Pallas kernels  102 us (98%)
    pallas_call x1, Pallas kernels, shards(): pl.pallas_call(functools.partial(kernel, groups, cap), out_shape=jax.Shap...  102 us

profile of v3, /device:TPU:0, one launch (start us, length us, event | category | flops | bytes accessed | tf_op | source)
XLA Modules:
  0.0 103.2 jit_solution(16464449031580725575)
XLA Ops:
  0.0 102.3 %shard_map.73 = bf16[256,2048]{1,0:T(8,128)(2,1)S(1)} custom-call(s32[2,256]{1,0:T(2,128)} %bitcast.4, f32[2,256]{1,0:T(2,128)} %bitcast.5, bf16[256,2048]{1,0:T(8,128)(2,1)} %tokens_hbm.1, f32[1,2048]{1,0:T(1,128)} %bitcast.3, bf16[1,2048,1024]{2,1,0:T(8,128)(2,1)} %wg_hbm.1, bf16[1,2048,1024]{2,1,0:T(8,128)(2,1)} %wu_hbm.1, bf16[1,1024,2048]{2,1,0:T(8,128)(2,1)} %wd_hbm.1), custom_call_target="tpu_custom_call" | custom-call | tf_op jit(solution)/shard_map/pallas_call | solution.py:410
  102.3 1.0 copy.9

commit v4 on v3

--- a/solution.py
+++ b/solution.py
@@ -45,7 +45,7 @@
     return order
 
 
-def plan(groups):
+def plan(groups, outer):
     upper, lower = halves(groups)
     near = [i for i in lower if bits(i) == 1]
     rest = [i for i in lower if bits(i) > 1]
@@ -65,16 +65,27 @@
     select(0, *near, upper[0])
     output(near[0])
     select(upper[1])
-    output(upper[0], *near[1:])
+    output(upper[0])
+    if outer:
+        select(*rest)
+    else:
+        output(*near[1:])
     for before, i in zip(upper[1:], upper[2:]):
         select(i)
         mix(1)
         output(before)
     mix(1)
-    select(*rest)
-    output(upper[-1])
-    mix(1)
-    output(*rest, 0)
+    if outer:
+        output(*rest, upper[-1])
+        mix(len(rest) + 1)
+        output(*near[1:])
+        mix(len(near))
+        output(0)
+    else:
+        select(*rest)
+        output(upper[-1])
+        mix(1)
+        output(*rest, 0)
     mix(0)
 
     rows, last = [], 2
@@ -352,12 +363,20 @@
                     comb[i, h, :, cols] = mixed(h, cols)
                 r1_copy(i, h).start()
 
-    selects, mixes, outputs = plan(groups)
-    first_output = next(t for t, i in enumerate(outputs) if i >= 0)
-
-    @pl.loop(0, len(selects))
+    plans = [plan(groups, False), plan(groups, True)]
+    length = max(len(p[0]) for p in plans)
+    outer = (group // (groups // 2)) % 2 == (group // (groups // 4)) % 2
+
+    def planned(kind, t):
+        inner_table, outer_table = (p[kind] + [-1] * (length - len(p[kind])) for p in plans)
+        return jnp.where(outer, entry(outer_table, t), entry(inner_table, t))
+
+    first_outputs = [next(t for t, i in enumerate(p[2]) if i >= 0) for p in plans]
+    first_output = jnp.where(outer, first_outputs[1], first_outputs[0])
+
+    @pl.loop(0, length)
     def _(t):
-        to_select, to_mix, to_output = entry(selects, t), entry(mixes, t), entry(outputs, t)
+        to_select, to_mix, to_output = planned(0, t), planned(1, t), planned(2, t)
 
         @pl.when(to_select >= 0)
         def _():

time: 104 us -> 102 us (0.981)
    pallas_call x1, Pallas kernels: 102 us -> 101 us  [shards(): pl.pallas_call(functools.partial(kernel, groups, cap), out_shape=jax.Shap...]
where the time goes in v4:
time: 102 us
  Pallas kernels  101 us (99%)
    pallas_call x1, Pallas kernels, shards(): pl.pallas_call(functools.partial(kernel, groups, cap), out_shape=jax.Shap...  101 us

profile of v4, /device:TPU:0, one launch (start us, length us, event | category | flops | bytes accessed | tf_op | source)
XLA Modules:
  0.0 101.9 jit_solution(4963066288944283701)
XLA Ops:
  0.0 100.9 %shard_map.73 = bf16[256,2048]{1,0:T(8,128)(2,1)S(1)} custom-call(s32[2,256]{1,0:T(2,128)} %bitcast.4, f32[2,256]{1,0:T(2,128)} %bitcast.5, bf16[256,2048]{1,0:T(8,128)(2,1)} %tokens_hbm.1, f32[1,2048]{1,0:T(1,128)} %bitcast.3, bf16[1,2048,1024]{2,1,0:T(8,128)(2,1)} %wg_hbm.1, bf16[1,2048,1024]{2,1,0:T(8,128)(2,1)} %wu_hbm.1, bf16[1,1024,2048]{2,1,0:T(8,128)(2,1)} %wd_hbm.1), custom_call_target="tpu_custom_call" | custom-call | tf_op jit(solution)/shard_map/pallas_call | solution.py:429
  100.9 1.0 copy.9

commit v5 on v4

--- a/solution.py
+++ b/solution.py
@@ -76,7 +76,7 @@
         output(before)
     mix(1)
     if outer:
-        output(*rest, upper[-1])
+        output(upper[-1], *rest)
         mix(len(rest) + 1)
         output(*near[1:])
         mix(len(near))
@@ -409,7 +409,7 @@
     landed(comb.at[1:], r1_send.at[0])
     landed(back.at[1:], r1_recv.at[0])
     for h in range(PARTS):
-        for cols in chunks(part, 512):
+        for cols in chunks(part, 256):
             target = pl.ds(h * part + cols.start, cols.stop - cols.start)
             out_ref[:, target] = dot(spread_ref[...], merge_rows(back[:, h, :, cols])).astype(BF16)
 

time: 102 us -> 102 us (level)
  no operation moved by 1% of the time
where the time goes in v5:
time: 102 us
  Pallas kernels  101 us (99%)
    pallas_call x1, Pallas kernels, shards(): pl.pallas_call(functools.partial(kernel, groups, cap), out_shape=jax.Shap...  101 us

profile of v5, /device:TPU:0, one launch (start us, length us, event | category | flops | bytes accessed | tf_op | source)
XLA Modules:
  0.0 101.9 jit_solution(1969126265470652834)
XLA Ops:
  0.0 100.9 %shard_map.73 = bf16[256,2048]{1,0:T(8,128)(2,1)S(1)} custom-call(s32[2,256]{1,0:T(2,128)} %bitcast.4, f32[2,256]{1,0:T(2,128)} %bitcast.5, bf16[256,2048]{1,0:T(8,128)(2,1)} %tokens_hbm.1, f32[1,2048]{1,0:T(1,128)} %bitcast.3, bf16[1,2048,1024]{2,1,0:T(8,128)(2,1)} %wg_hbm.1, bf16[1,2048,1024]{2,1,0:T(8,128)(2,1)} %wu_hbm.1, bf16[1,1024,2048]{2,1,0:T(8,128)(2,1)} %wd_hbm.1), custom_call_target="tpu_custom_call" | custom-call | tf_op jit(solution)/shard_map/pallas_call | solution.py:429
  100.9 1.0 copy.9
